TPU v7x, 128 devices: a whole 4x4x4 slice. The times are simulated.
128 devices in a mesh: rep: 2 (over x_hi), fs: 16 (over y, x_lo, core), tp: 4 (over z).
Axes of the slice: x: 4 (x_hi: 2, x_lo: 2; x = x_hi * 2 + x_lo), y: 4, z: 4, core: 2. Of those that a mesh axis runs over, the one named last changes fastest.
Arguments:
- tokens: bfloat16 [16384, 2048], P(('rep', 'fs', 'tp')), may hold values from -3 to 3
- mixer_output: bfloat16 [16384, 2048], P(('rep', 'fs', 'tp')), may hold values from -6 to 6
- early_norm: float32 [2048], replicated, may hold values from 0.75 to 1.25
- early_gate: bfloat16 [2048, 5120], P('fs', 'tp'), may hold values from -0.125 to 0.125
- early_value: bfloat16 [2048, 5120], P('fs', 'tp'), may hold values from -0.125 to 0.125
- early_down: bfloat16 [5120, 2048], P('tp', 'fs'), may hold values from -0.078125 to 0.078125
- early_post: float32 [2048], replicated, may hold values from 0.75 to 1.25
- mixer_gain: float32 [2048], replicated, may hold values from 0.75 to 1.25
- later_norm: float32 [2048], replicated, may hold values from 0.75 to 1.25
- later_gate: bfloat16 [2048, 5120], P('fs', 'tp'), may hold values from -0.125 to 0.125
- later_value: bfloat16 [2048, 5120], P('fs', 'tp'), may hold values from -0.125 to 0.125
- later_down: bfloat16 [5120, 2048], P('tp', 'fs'), may hold values from -0.078125 to 0.078125
- later_post: float32 [2048], replicated, may hold values from 0.75 to 1.25
Outputs:
- layer_out: bfloat16 [16384, 2048], P(('rep', 'fs', 'tp'))
All inputs are finite; a program needn't handle non-finite values.
Results may differ from a plain program's by a relative error of at most 0.015.
Values may be sent and summed in bfloat16 or wider, within the bound.
A program may use at most 128 MiB of HBM per device.

v0:
```python
import jax
import jax.numpy as jnp
from jax import lax
from jax.sharding import PartitionSpec as P

epsilon = 1e-06


def over_all(piece, axis, dim, step, start):

    def gathered(part):
        return lax.all_gather(part, axis, axis=dim, tiled=True)

    return step(start, jax.tree.map(gathered, piece), jnp.int32(0))


def own_rows(product, extent, axis):
    everything = product(jnp.int32(0), lax.axis_size(axis) * extent)
    own = lax.psum_scatter(everything.astype(jnp.bfloat16), axis, scatter_dimension=0, tiled=True)
    return own.astype(jnp.float32)


def rms_scale(values, gain):
    values = values.astype(jnp.float32)
    scale = lax.rsqrt(jnp.mean(values * values, axis=-1, keepdims=True) + epsilon)
    return values * scale * gain


def half_branch(normed, gate_piece, value_piece, down_piece):
    all_rows = lax.all_gather(normed, "tp", axis=0, tiled=True)
    empty = jnp.zeros((all_rows.shape[0], gate_piece.shape[1]), jnp.float32)

    def add_rows(totals, pieces, start):
        columns = lax.dynamic_slice_in_dim(all_rows, start, pieces[0].shape[0], 1)
        gate_part = jnp.dot(columns, pieces[0], preferred_element_type=jnp.float32)
        value_part = jnp.dot(columns, pieces[1], preferred_element_type=jnp.float32)
        return (totals[0] + gate_part, totals[1] + value_part)

    gate_sum, value_sum = over_all((gate_piece, value_piece), "fs", 0, add_rows, (empty, empty))
    down_block = lax.all_gather(down_piece, "fs", axis=1, tiled=True)
    hidden = (jax.nn.silu(gate_sum) * value_sum).astype(jnp.bfloat16)

    def row_term(start, count):
        rows = lax.dynamic_slice_in_dim(hidden, start, count, 0)
        return jnp.dot(rows, down_block, preferred_element_type=jnp.float32)

    return own_rows(row_term, normed.shape[0], "tp")


def on_device(
    tokens,
    mixer_output,
    early_norm,
    early_gate,
    early_value,
    early_down,
    early_post,
    mixer_gain,
    later_norm,
    later_gate,
    later_value,
    later_down,
    later_post,
):
    early_in = rms_scale(tokens, early_norm).astype(jnp.bfloat16)
    early_branch = half_branch(early_in, early_gate, early_value, early_down)
    mixed = (
        tokens.astype(jnp.float32)
        + 0.5 * rms_scale(early_branch, early_post)
        + rms_scale(mixer_output, mixer_gain)
    )
    mixed = mixed.astype(jnp.bfloat16)
    later_in = rms_scale(mixed, later_norm).astype(jnp.bfloat16)
    later_branch = half_branch(later_in, later_gate, later_value, later_down)
    layer_out = mixed.astype(jnp.float32) + 0.5 * rms_scale(later_branch, later_post)
    return layer_out.astype(jnp.bfloat16)


def solution(mesh):
    placed = (
        P(("rep", "fs", "tp"), None),
        P(("rep", "fs", "tp"), None),
        P(),
        P("fs", "tp"),
        P("fs", "tp"),
        P("tp", "fs"),
        P(),
        P(),
        P(),
        P("fs", "tp"),
        P("fs", "tp"),
        P("tp", "fs"),
        P(),
    )
    return jax.shard_map(
        on_device,
        mesh=mesh,
        in_specs=placed,
        out_specs=P(("rep", "fs", "tp"), None),
        check_vma=False,
    )
```

profile of v0, /device:TPU:1, one launch (start us, length us, event | category | flops | bytes accessed | tf_op | source)
XLA Modules:
  0.0 438.2 jit_solution(11551723246681318497)
XLA Ops:
  6.5 1.2 fusion.12
  7.8 2.0 fusion.14
  9.8 0.0 all-gather.11.cloned.1.call-start
  9.9 0.7 all-gather.11.cloned.1.call-update
  10.6 0.7 all-gather.13.cloned.1.call-update
  11.4 0.5 all-gather.15.cloned.1.call-update
  11.9 32.1 %all-gather.9.cloned.1.call-done = bf16[512,2048]{1,0:T(8,128)(2,1)} async-done(((bf16[128,2048]{1,0:T(8,128)(2,1)}), bf16[512,2048]{1,0:T(8,128)(2,1)}) %all-gather.9.cloned.1.call-update) | async-done | bytes 2097168 | tf_op jit(solution)/shard_map/all_gather | solution.py:30
  44.0 41.1 %all-gather.11.cloned.1.call-done = bf16[2048,1280]{1,0:T(8,128)(2,1)} async-done(((bf16[128,1280]{1,0:T(8,128)(2,1)}), bf16[2048,1280]{1,0:T(8,128)(2,1)}) %all-gather.11.cloned.1.call-update) | async-done | bytes 5242896 | tf_op jit(solution)/shard_map/all_gather | solution.py:12
  85.1 7.5 %fusion.22 = f32[512,1280]{1,0:T(8,128)} fusion(bf16[512,2048]{1,0:T(8,128)(2,1)} %all-gather.9.cloned.1.call-done, bf16[2048,1280]{1,0:T(8,128)(2,1)} %all-gather.11.cloned.1.call-done), kind=kOutput, calls=%fused_computation.42 | convolution fusion | flops 2684354560 | bytes 9961472 | tf_op jit(solution)/shard_map/dot_general | solution.py:35
  92.6 33.7 %all-gather.13.cloned.1.call-done = bf16[2048,1280]{1,0:T(8,128)(2,1)} async-done(((bf16[128,1280]{1,0:T(8,128)(2,1)}), bf16[2048,1280]{1,0:T(8,128)(2,1)}) %all-gather.13.cloned.1.call-update) | async-done | bytes 5242896 | tf_op jit(solution)/shard_map/all_gather | solution.py:12
  126.3 51.5 %all-gather.15.cloned.1.call-done = bf16[1280,2048]{1,0:T(8,128)(2,1)} async-done(((bf16[1280,128]{1,0:T(8,128)(2,1)}), bf16[1280,2048]{1,0:T(8,128)(2,1)}) %all-gather.15.cloned.1.call-update) | async-done | bytes 5242896 | tf_op jit(solution)/shard_map/all_gather | solution.py:40
  177.8 12.5 %convolution_convert_fusion.1 = bf16[512,2048]{1,0:T(8,128)(2,1)} fusion(bf16[1280,2048]{1,0:T(8,128)(2,1)} %all-gather.15.cloned.1.call-done, bf16[512,2048]{1,0:T(8,128)(2,1)S(1)} %copy-done.6, bf16[2048,1280]{1,0:T(8,128)(2,1)} %all-gather.13.cloned.1.call-done, f32[512,1280]{1,0:T(8,128)} %fusion.22), kind=kOutput, calls=%fused_computation.5 | convolution fusion | flops 5373689856 | bytes 17301504 | tf_op jit(solution)/shard_map/dot_general | solution.py:45
  190.4 0.5 all-gather.19.cloned.1.call-update
  190.9 0.4 copy-done.1
  191.3 0.2 fusion.5
  191.5 28.4 %reduce-scatter.3.cloned.1.call-done = bf16[128,2048]{1,0:T(8,128)(2,1)} async-done(((bf16[512,2048]{1,0:T(8,128)(2,1)}), bf16[128,2048]{1,0:T(8,128)(2,1)}) %reduce-scatter.3.cloned.1.call-update) | async-done | bytes 524304 | tf_op jit(solution)/shard_map/reduce_scatter | solution.py:19
  219.9 1.2 fusion.2
  221.2 1.6 fusion.15
  222.8 1.0 fusion.17
  223.8 0.0 all-gather.21.cloned.1.call-start
  223.9 0.7 all-gather.21.cloned.1.call-update
  224.6 0.7 all-gather.23.cloned.1.call-update
  225.3 0.2 reduce-scatter.5.cloned.1.call-start
  225.6 34.9 %all-gather.19.cloned.1.call-done = bf16[2048,1280]{1,0:T(8,128)(2,1)} async-done(((bf16[128,1280]{1,0:T(8,128)(2,1)}), bf16[2048,1280]{1,0:T(8,128)(2,1)}) %all-gather.19.cloned.1.call-update) | async-done | bytes 5242896 | tf_op jit(solution)/shard_map/all_gather | solution.py:12
  260.5 32.6 %all-gather.17.cloned.1.call-done = bf16[512,2048]{1,0:T(8,128)(2,1)} async-done(((bf16[128,2048]{1,0:T(8,128)(2,1)}), bf16[512,2048]{1,0:T(8,128)(2,1)}) %all-gather.17.cloned.1.call-update) | async-done | bytes 2097168 | tf_op jit(solution)/shard_map/all_gather | solution.py:30
  293.1 7.6 %fusion.23 = f32[512,1280]{1,0:T(8,128)} fusion(bf16[512,2048]{1,0:T(8,128)(2,1)} %all-gather.17.cloned.1.call-done, bf16[2048,1280]{1,0:T(8,128)(2,1)} %all-gather.19.cloned.1.call-done), kind=kOutput, calls=%fused_computation.43 | convolution fusion | flops 2684354560 | bytes 9961472 | tf_op jit(solution)/shard_map/dot_general | solution.py:35
  300.8 33.5 %all-gather.21.cloned.1.call-done = bf16[2048,1280]{1,0:T(8,128)(2,1)} async-done(((bf16[128,1280]{1,0:T(8,128)(2,1)}), bf16[2048,1280]{1,0:T(8,128)(2,1)}) %all-gather.21.cloned.1.call-update) | async-done | bytes 5242896 | tf_op jit(solution)/shard_map/all_gather | solution.py:12
  334.2 51.6 %all-gather.23.cloned.1.call-done = bf16[1280,2048]{1,0:T(8,128)(2,1)} async-done(((bf16[1280,128]{1,0:T(8,128)(2,1)}), bf16[1280,2048]{1,0:T(8,128)(2,1)}) %all-gather.23.cloned.1.call-update) | async-done | bytes 5242896 | tf_op jit(solution)/shard_map/all_gather | solution.py:40
  385.9 12.5 %convolution_convert_fusion = bf16[512,2048]{1,0:T(8,128)(2,1)} fusion(bf16[1280,2048]{1,0:T(8,128)(2,1)} %all-gather.23.cloned.1.call-done, bf16[512,2048]{1,0:T(8,128)(2,1)S(1)} %copy-done.7, bf16[2048,1280]{1,0:T(8,128)(2,1)} %all-gather.21.cloned.1.call-done, f32[512,1280]{1,0:T(8,128)} %fusion.23), kind=kOutput, calls=%fused_computation.4 | convolution fusion | flops 5373689856 | bytes 17301504 | tf_op jit(solution)/shard_map/dot_general | solution.py:45
  398.4 29.6 %reduce-scatter.5.cloned.1.call-done = bf16[128,2048]{1,0:T(8,128)(2,1)} async-done(((bf16[512,2048]{1,0:T(8,128)(2,1)}), bf16[128,2048]{1,0:T(8,128)(2,1)}) %reduce-scatter.5.cloned.1.call-update) | async-done | bytes 524304 | tf_op jit(solution)/shard_map/reduce_scatter | solution.py:19
  428.0 1.2 fusion.9
  429.2 2.1 fusion.18
  (31 shorter events, 0.4 us)
Async XLA Ops:
  6.5 37.5 %all-gather.9.cloned.1.call-start = ((), (), s32[]{:S(2)}) async-start(), calls=%async_computation.2 | async-start | bytes 2621440 | tf_op jit(solution)/shard_map/all_gather | solution.py:30
  9.8 75.3 %all-gather.11.cloned.1.call-start = ((), (), s32[]{:S(2)}) async-start(), calls=%async_computation.3 | async-start | bytes 5570560 | tf_op jit(solution)/shard_map/all_gather | solution.py:12
  10.6 115.7 %all-gather.13.cloned.1.call-start = ((), (), s32[]{:S(2)}) async-start(), calls=%async_computation.4 | async-start | bytes 5570560 | tf_op jit(solution)/shard_map/all_gather | solution.py:12
  11.3 166.5 %all-gather.15.cloned.1.call-start = ((), (), s32[]{:S(2)}) async-start(), calls=%async_computation.5 | async-start | bytes 5570560 | tf_op jit(solution)/shard_map/all_gather | solution.py:40
  11.9 208.0 %reduce-scatter.3.cloned.1.call-start = ((), (), s32[]{:S(2)}) async-start(), calls=%async_computation.6 | async-start | bytes 2621440 | tf_op jit(solution)/shard_map/reduce_scatter | solution.py:19
  44.0 133.8 %copy-start.6 = (bf16[512,2048]{1,0:T(8,128)(2,1)S(1)}, bf16[512,2048]{1,0:T(8,128)(2,1)}, u32[]{:S(2)}) copy-start(bf16[512,2048]{1,0:T(8,128)(2,1)} %all-gather.9.cloned.1.call-done) | copy-start | bytes 6291460
  190.3 1.0 copy-start.1
  190.3 30.9 %copy-start = (bf16[128,2048]{1,0:T(8,128)(2,1)S(1)}, bf16[128,2048]{1,0:T(8,128)(2,1)}, u32[]{:S(2)}) copy-start(bf16[128,2048]{1,0:T(8,128)(2,1)} %param.13) | copy-start | bytes 1572868
  190.3 30.9 %copy-start.2 = (f32[2048]{0:T(1024)S(1)}, f32[2048]{0:T(1024)}, u32[]{:S(2)}) copy-start(f32[2048]{0:T(1024)} %param.20) | copy-start | bytes 24580
  190.3 30.9 %copy-start.3 = (f32[2048]{0:T(1024)S(1)}, f32[2048]{0:T(1024)}, u32[]{:S(2)}) copy-start(f32[2048]{0:T(1024)} %param.19) | copy-start | bytes 24580
  190.3 32.6 %copy-start.4 = (f32[2048]{0:T(1024)S(1)}, f32[2048]{0:T(1024)}, u32[]{:S(2)}) copy-start(f32[2048]{0:T(1024)} %param.21) | copy-start | bytes 24580
  190.3 70.2 %all-gather.19.cloned.1.call-start = ((), (), s32[]{:S(2)}) async-start(), calls=%async_computation.8 | async-start | bytes 5570560 | tf_op jit(solution)/shard_map/all_gather | solution.py:12
  190.9 102.2 %all-gather.17.cloned.1.call-start = ((), (), s32[]{:S(2)}) async-start(), calls=%async_computation.7 | async-start | bytes 2621440 | tf_op jit(solution)/shard_map/all_gather | solution.py:30
  223.8 110.4 %all-gather.21.cloned.1.call-start = ((), (), s32[]{:S(2)}) async-start(), calls=%async_computation.9 | async-start | bytes 5570560 | tf_op jit(solution)/shard_map/all_gather | solution.py:12
  224.6 161.2 %all-gather.23.cloned.1.call-start = ((), (), s32[]{:S(2)}) async-start(), calls=%async_computation.10 | async-start | bytes 5570560 | tf_op jit(solution)/shard_map/all_gather | solution.py:40
  225.3 202.7 %reduce-scatter.5.cloned.1.call-start = ((), (), s32[]{:S(2)}) async-start(), calls=%async_computation.11 | async-start | bytes 2621440 | tf_op jit(solution)/shard_map/reduce_scatter | solution.py:19
  293.1 92.7 %copy-start.7 = (bf16[512,2048]{1,0:T(8,128)(2,1)S(1)}, bf16[512,2048]{1,0:T(8,128)(2,1)}, u32[]{:S(2)}) copy-start(bf16[512,2048]{1,0:T(8,128)(2,1)} %all-gather.17.cloned.1.call-done) | copy-start | bytes 6291460
  398.3 30.9 %copy-start.5 = (f32[2048]{0:T(1024)S(1)}, f32[2048]{0:T(1024)}, u32[]{:S(2)}) copy-start(f32[2048]{0:T(1024)} %param.25) | copy-start | bytes 24580
Sparse Core Ops, SparseCore 0:
  9.9 34.0 all-gather.8
  45.7 39.3 all-gather.10
  86.8 39.4 all-gather.12
  127.8 49.9 all-gather.14
  190.4 29.4 reduce-scatter.2
  221.5 38.9 all-gather.18
  262.2 30.9 all-gather.16
  294.8 39.3 all-gather.20
  335.9 49.9 all-gather.22
  398.5 29.4 reduce-scatter.4
where the time goes:
time: 439 us; the launch traced here: 438 us
  waiting for transfers between devices  373 us (85%)
  matrix products  40.1 us (9%)
  between operations  13.6 us (3%)
  other arithmetic  10.7 us (2%)
    all_gather x4, waiting for transfers between devices, gathered(): return lax.all_gather(part, axis, axis=dim, tiled=True)  143 us
    all_gather x2, waiting for transfers between devices, half_branch(): down_block = lax.all_gather(down_piece, 'fs', axis=1, tiled=True)  103 us
    all_gather x2, waiting for transfers between devices, half_branch(): all_rows = lax.all_gather(normed, 'tp', axis=0, tiled=True)  64.7 us
    reduce_scatter x2, waiting for transfers between devices, own_rows(): lax.psum_scatter(everything.astype(jnp.bfloat16), axis, scatter_dimension...  58.1 us
    dot_general x2, matrix products, row_term(): return jnp.dot(rows, down_block, preferred_element_type=jnp.float32)  25 us
    dot_general x2, matrix products, add_rows(): gate_part = jnp.dot(columns, pieces[0], preferred_element_type=jnp.float32)  15.1 us
  transfers between devices with their start and end apart: 10, of which 10 were waited for; matrix products, arithmetic and copies ran while one was open for 4% of the time, Pallas kernels for 0%

commit v1 on v0

--- a/solution.py
+++ b/solution.py
@@ -1,9 +1,18 @@
+import functools
 import jax
 import jax.numpy as jnp
 from jax import lax
 from jax.sharding import PartitionSpec as P
 
 epsilon = 1e-06
+
+
+def begin_the_streams(mat, bus_axis):
+    mat_out = jnp.concatenate(lax.all_gather(mat, axis_name=bus_axis), axis=1)
+    return mat_out
+
+
+watch_fields = functools.partial(begin_the_streams, bus_axis="fs")
 
 
 def over_all(piece, axis, dim, step, start):
@@ -37,7 +46,7 @@
         return (totals[0] + gate_part, totals[1] + value_part)
 
     gate_sum, value_sum = over_all((gate_piece, value_piece), "fs", 0, add_rows, (empty, empty))
-    down_block = lax.all_gather(down_piece, "fs", axis=1, tiled=True)
+    down_block = watch_fields(down_piece)
     hidden = (jax.nn.silu(gate_sum) * value_sum).astype(jnp.bfloat16)
 
     def row_term(start, count):

time: 439 us -> 418 us (0.952)
  waiting for transfers between devices: 373 us -> 337 us
  local copies, waits for them, and re-layouts: 0.39 us -> 15.7 us
    all_gather x2, waiting for transfers between devices: 103 us -> 75.3 us  [begin_the_streams(): mat_out = jnp.concatenate(lax.all_gather(mat, axis_name=bus_axis), axis=1)]
    reshape x0 -> x2, local copies, waits for them, and re-layouts: none -> 15.7 us  [begin_the_streams(): mat_out = jnp.concatenate(lax.all_gather(mat, axis_name=bus_axis), axis=1)]
    all_gather x2, waiting for transfers between devices: 64.7 us -> 57.4 us  [half_branch(): all_rows = lax.all_gather(normed, 'tp', axis=0, tiled=True)]
  transfers between devices with their start and end apart: 10 -> 10, of which waited for: 10 -> 10; matrix products, arithmetic and copies ran while one was open for 4% -> 9% of each run, Pallas kernels for 0% -> 0%
where the time goes in v1:
time: 418 us; the launch traced here: 417 us
  waiting for transfers between devices  337 us (81%)
  matrix products  40.2 us (10%)
  local copies, waits for them, and re-layouts  15.7 us (4%)
  between operations  13.6 us (3%)
  other arithmetic  10.7 us (3%)
    all_gather x4, waiting for transfers between devices, gathered(): return lax.all_gather(part, axis, axis=dim, tiled=True)  141 us
    all_gather x2, waiting for transfers between devices, begin_the_streams(): mat_out = jnp.concatenate(lax.all_gather(mat, axis_name=bus_axis), axis=1)  75.3 us
    reduce_scatter x2, waiting for transfers between devices, own_rows(): lax.psum_scatter(everything.astype(jnp.bfloat16), axis, scatter_dimension...  58.7 us
    all_gather x2, waiting for transfers between devices, half_branch(): all_rows = lax.all_gather(normed, 'tp', axis=0, tiled=True)  57.4 us
    dot_general x2, matrix products, row_term(): return jnp.dot(rows, down_block, preferred_element_type=jnp.float32)  24.9 us
    reshape x2, local copies, waits for them, and re-layouts, begin_the_streams(): mat_out = jnp.concatenate(lax.all_gather(mat, axis_name=bus_axis), axis=1)  15.7 us
    dot_general x2, matrix products, add_rows(): gate_part = jnp.dot(columns, pieces[0], preferred_element_type=jnp.float32)  15.2 us
  transfers between devices with their start and end apart: 10, of which 10 were waited for; matrix products, arithmetic and copies ran while one was open for 9% of the time, Pallas kernels for 0%

profile of v1, /device:TPU:1, one launch (start us, length us, event | category | flops | bytes accessed | tf_op | source)
XLA Modules:
  0.0 417.4 jit_solution(10717617154942271827)
XLA Ops:
  6.5 0.7 all-gather.23.cloned.1.call-update
  7.3 1.2 fusion.12
  8.5 2.0 fusion.14
  10.6 0.0 all-gather.13.cloned.1.call-start
  10.6 0.7 all-gather.13.cloned.1.call-update
  11.4 0.5 all-gather.15.cloned.1.call-update
  12.0 39.6 %all-gather.23.cloned.1.call-done = bf16[20480,128]{1,0:T(8,128)(2,1)} async-done(((bf16[1280,128]{1,0:T(8,128)(2,1)}), bf16[20480,128]{1,0:T(8,128)(2,1)}) %all-gather.23.cloned.1.call-update) | async-done | bytes 5242896 | tf_op jit(solution)/shard_map/all_gather | solution.py:11
  51.6 7.9 %copy.14 = bf16[1280,16,128]{0,2,1:T(8,128)(2,1)} copy(bf16[1280,16,128]{2,0,1:T(8,128)(2,1)} %bitcast.19) | data formatting | bytes 10485760 | tf_op jit(solution)/shard_map/reshape | solution.py:11
  59.5 24.7 %all-gather.11.cloned.1.call-done = bf16[512,2048]{1,0:T(8,128)(2,1)} async-done(((bf16[128,2048]{1,0:T(8,128)(2,1)}), bf16[512,2048]{1,0:T(8,128)(2,1)}) %all-gather.11.cloned.1.call-update) | async-done | bytes 2097168 | tf_op jit(solution)/shard_map/all_gather | solution.py:39
  84.2 41.1 %all-gather.13.cloned.1.call-done = bf16[2048,1280]{1,0:T(8,128)(2,1)} async-done(((bf16[128,1280]{1,0:T(8,128)(2,1)}), bf16[2048,1280]{1,0:T(8,128)(2,1)}) %all-gather.13.cloned.1.call-update) | async-done | bytes 5242896 | tf_op jit(solution)/shard_map/all_gather | solution.py:21
  125.4 7.5 %fusion.22 = f32[512,1280]{1,0:T(8,128)} fusion(bf16[512,2048]{1,0:T(8,128)(2,1)} %all-gather.11.cloned.1.call-done, bf16[2048,1280]{1,0:T(8,128)(2,1)} %all-gather.13.cloned.1.call-done), kind=kOutput, calls=%fused_computation.42 | convolution fusion | flops 2684354560 | bytes 9961472 | tf_op jit(solution)/shard_map/dot_general | solution.py:44
  132.9 33.5 %all-gather.15.cloned.1.call-done = bf16[2048,1280]{1,0:T(8,128)(2,1)} async-done(((bf16[128,1280]{1,0:T(8,128)(2,1)}), bf16[2048,1280]{1,0:T(8,128)(2,1)}) %all-gather.15.cloned.1.call-update) | async-done | bytes 5242896 | tf_op jit(solution)/shard_map/all_gather | solution.py:21
  166.4 12.5 %convolution_convert_fusion.1 = bf16[512,2048]{1,0:T(8,128)(2,1)} fusion(bf16[1280,2048]{0,1:T(8,128)(2,1)} %bitcast.20, bf16[512,2048]{1,0:T(8,128)(2,1)S(1)} %copy-done.6, bf16[2048,1280]{1,0:T(8,128)(2,1)} %all-gather.15.cloned.1.call-done, f32[512,1280]{1,0:T(8,128)} %fusion.22), kind=kOutput, calls=%fused_computation.5 | convolution fusion | flops 5373689856 | bytes 17301504 | tf_op jit(solution)/shard_map/dot_general | solution.py:54
  179.0 0.5 all-gather.25.cloned.1.call-update
  179.6 0.7 all-gather.19.cloned.1.call-update
  180.3 0.2 fusion.5
  180.5 28.5 %reduce-scatter.3.cloned.1.call-done = bf16[128,2048]{1,0:T(8,128)(2,1)} async-done(((bf16[512,2048]{1,0:T(8,128)(2,1)}), bf16[128,2048]{1,0:T(8,128)(2,1)}) %reduce-scatter.3.cloned.1.call-update) | async-done | bytes 524304 | tf_op jit(solution)/shard_map/reduce_scatter | solution.py:28
  209.1 1.2 fusion.2
  210.3 1.6 fusion.15
  212.0 1.0 fusion.17
  213.0 0.7 all-gather.21.cloned.1.call-update
  213.7 0.2 reduce-scatter.5.cloned.1.call-start
  213.9 35.7 %all-gather.25.cloned.1.call-done = bf16[20480,128]{1,0:T(8,128)(2,1)} async-done(((bf16[1280,128]{1,0:T(8,128)(2,1)}), bf16[20480,128]{1,0:T(8,128)(2,1)}) %all-gather.25.cloned.1.call-update) | async-done | bytes 5242896 | tf_op jit(solution)/shard_map/all_gather | solution.py:11
  249.6 7.8 %copy.15 = bf16[1280,16,128]{0,2,1:T(8,128)(2,1)} copy(bf16[1280,16,128]{2,0,1:T(8,128)(2,1)} %bitcast.18) | data formatting | bytes 10485760 | tf_op jit(solution)/shard_map/reshape | solution.py:11
  257.4 33.4 %all-gather.19.cloned.1.call-done = bf16[2048,1280]{1,0:T(8,128)(2,1)} async-done(((bf16[128,1280]{1,0:T(8,128)(2,1)}), bf16[2048,1280]{1,0:T(8,128)(2,1)}) %all-gather.19.cloned.1.call-update) | async-done | bytes 5242896 | tf_op jit(solution)/shard_map/all_gather | solution.py:21
  290.8 32.6 %all-gather.17.cloned.1.call-done = bf16[512,2048]{1,0:T(8,128)(2,1)} async-done(((bf16[128,2048]{1,0:T(8,128)(2,1)}), bf16[512,2048]{1,0:T(8,128)(2,1)}) %all-gather.17.cloned.1.call-update) | async-done | bytes 2097168 | tf_op jit(solution)/shard_map/all_gather | solution.py:39
  323.5 7.7 %fusion.23 = f32[512,1280]{1,0:T(8,128)} fusion(bf16[512,2048]{1,0:T(8,128)(2,1)} %all-gather.17.cloned.1.call-done, bf16[2048,1280]{1,0:T(8,128)(2,1)} %all-gather.19.cloned.1.call-done), kind=kOutput, calls=%fused_computation.43 | convolution fusion | flops 2684354560 | bytes 9961472 | tf_op jit(solution)/shard_map/dot_general | solution.py:44
  331.2 33.4 %all-gather.21.cloned.1.call-done = bf16[2048,1280]{1,0:T(8,128)(2,1)} async-done(((bf16[128,1280]{1,0:T(8,128)(2,1)}), bf16[2048,1280]{1,0:T(8,128)(2,1)}) %all-gather.21.cloned.1.call-update) | async-done | bytes 5242896 | tf_op jit(solution)/shard_map/all_gather | solution.py:21
  364.6 12.5 %convolution_convert_fusion = bf16[512,2048]{1,0:T(8,128)(2,1)} fusion(bf16[1280,2048]{0,1:T(8,128)(2,1)} %bitcast.21, bf16[512,2048]{1,0:T(8,128)(2,1)S(1)} %copy-done.7, bf16[2048,1280]{1,0:T(8,128)(2,1)} %all-gather.21.cloned.1.call-done, f32[512,1280]{1,0:T(8,128)} %fusion.23), kind=kOutput, calls=%fused_computation.4 | convolution fusion | flops 5373689856 | bytes 17301504 | tf_op jit(solution)/shard_map/dot_general | solution.py:54
  377.1 30.1 %reduce-scatter.5.cloned.1.call-done = bf16[128,2048]{1,0:T(8,128)(2,1)} async-done(((bf16[512,2048]{1,0:T(8,128)(2,1)}), bf16[128,2048]{1,0:T(8,128)(2,1)}) %reduce-scatter.5.cloned.1.call-update) | async-done | bytes 524304 | tf_op jit(solution)/shard_map/reduce_scatter | solution.py:28
  407.2 1.2 fusion.9
  408.4 2.1 fusion.18
  (33 shorter events, 0.4 us)
Async XLA Ops:
  6.5 45.1 %all-gather.23.cloned.1.call-start = ((), (), s32[]{:S(2)}) async-start(), calls=%async_computation.10 | async-start | bytes 5570560 | tf_op jit(solution)/shard_map/all_gather | solution.py:11
  7.3 77.0 %all-gather.11.cloned.1.call-start = ((), (), s32[]{:S(2)}) async-start(), calls=%async_computation.2 | async-start | bytes 2621440 | tf_op jit(solution)/shard_map/all_gather | solution.py:39
  10.6 114.8 %all-gather.13.cloned.1.call-start = ((), (), s32[]{:S(2)}) async-start(), calls=%async_computation.3 | async-start | bytes 5570560 | tf_op jit(solution)/shard_map/all_gather | solution.py:21
  11.3 155.1 %all-gather.15.cloned.1.call-start = ((), (), s32[]{:S(2)}) async-start(), calls=%async_computation.4 | async-start | bytes 5570560 | tf_op jit(solution)/shard_map/all_gather | solution.py:21
  11.9 197.2 %reduce-scatter.3.cloned.1.call-start = ((), (), s32[]{:S(2)}) async-start(), calls=%async_computation.5 | async-start | bytes 2621440 | tf_op jit(solution)/shard_map/reduce_scatter | solution.py:28
  84.2 82.2 %copy-start.6 = (bf16[512,2048]{1,0:T(8,128)(2,1)S(1)}, bf16[512,2048]{1,0:T(8,128)(2,1)}, u32[]{:S(2)}) copy-start(bf16[512,2048]{1,0:T(8,128)(2,1)} %all-gather.11.cloned.1.call-done) | copy-start | bytes 6291460
  178.9 1.4 copy-start.1
  178.9 31.4 %copy-start = (bf16[128,2048]{1,0:T(8,128)(2,1)S(1)}, bf16[128,2048]{1,0:T(8,128)(2,1)}, u32[]{:S(2)}) copy-start(bf16[128,2048]{1,0:T(8,128)(2,1)} %param.13) | copy-start | bytes 1572868
  178.9 31.4 %copy-start.2 = (f32[2048]{0:T(1024)S(1)}, f32[2048]{0:T(1024)}, u32[]{:S(2)}) copy-start(f32[2048]{0:T(1024)} %param.20) | copy-start | bytes 24580
  178.9 31.4 %copy-start.3 = (f32[2048]{0:T(1024)S(1)}, f32[2048]{0:T(1024)}, u32[]{:S(2)}) copy-start(f32[2048]{0:T(1024)} %param.19) | copy-start | bytes 24580
  178.9 33.1 %copy-start.4 = (f32[2048]{0:T(1024)S(1)}, f32[2048]{0:T(1024)}, u32[]{:S(2)}) copy-start(f32[2048]{0:T(1024)} %param.21) | copy-start | bytes 24580
  178.9 70.7 %all-gather.25.cloned.1.call-start = ((), (), s32[]{:S(2)}) async-start(), calls=%async_computation.11 | async-start | bytes 5570560 | tf_op jit(solution)/shard_map/all_gather | solution.py:11
  179.5 111.3 %all-gather.19.cloned.1.call-start = ((), (), s32[]{:S(2)}) async-start(), calls=%async_computation.7 | async-start | bytes 5570560 | tf_op jit(solution)/shard_map/all_gather | solution.py:21
  180.3 143.2 %all-gather.17.cloned.1.call-start = ((), (), s32[]{:S(2)}) async-start(), calls=%async_computation.6 | async-start | bytes 2621440 | tf_op jit(solution)/shard_map/all_gather | solution.py:39
  213.0 151.6 %all-gather.21.cloned.1.call-start = ((), (), s32[]{:S(2)}) async-start(), calls=%async_computation.8 | async-start | bytes 5570560 | tf_op jit(solution)/shard_map/all_gather | solution.py:21
  213.7 193.5 %reduce-scatter.5.cloned.1.call-start = ((), (), s32[]{:S(2)}) async-start(), calls=%async_computation.9 | async-start | bytes 2621440 | tf_op jit(solution)/shard_map/reduce_scatter | solution.py:28
  323.5 41.1 %copy-start.7 = (bf16[512,2048]{1,0:T(8,128)(2,1)S(1)}, bf16[512,2048]{1,0:T(8,128)(2,1)}, u32[]{:S(2)}) copy-start(bf16[512,2048]{1,0:T(8,128)(2,1)} %all-gather.17.cloned.1.call-done) | copy-start | bytes 6291460
  377.1 31.4 %copy-start.5 = (f32[2048]{0:T(1024)S(1)}, f32[2048]{0:T(1024)}, u32[]{:S(2)}) copy-start(f32[2048]{0:T(1024)} %param.25) | copy-start | bytes 24580
Sparse Core Ops, SparseCore 0:
  9.0 42.5 all-gather.22
  53.3 30.9 all-gather.10
  86.0 39.3 all-gather.12
  126.9 39.4 all-gather.14
  179.1 29.9 reduce-scatter.2
  210.6 38.9 all-gather.24
  251.3 39.4 all-gather.18
  292.5 30.9 all-gather.16
  325.2 39.3 all-gather.20
  377.2 29.9 reduce-scatter.4
